TPU v7x, 32 devices: a whole 2x2x4 slice. The times are simulated.
32 devices in a mesh: sp: 16 (over z, y, x), tp: 2 (over core).
Axes of the slice: x: 2, y: 2, z: 4, core: 2. Of those that a mesh axis runs over, the one named last changes fastest.
Arguments:
- resid: bfloat16 [4096, 2048], P(('sp', 'tp')), may hold values from -6 to 6
- queries: bfloat16 [4096, 2048], P('sp', 'tp'), may hold values from -6 to 6
- keys: bfloat16 [4096, 1024], P('sp', 'tp'), may hold values from -6 to 6
- values: bfloat16 [4096, 1024], P('sp', 'tp'), may hold values from -6 to 6
- log_gates: float32 [16, 4096], P('tp'), as said below
- documents: int32 [4096], P('sp'), may hold values from 0 to 2, never falling along the last dimension, each value on 1 to 3072 neighbouring positions
- out_weight: bfloat16 [2048, 2048], P('tp'), may hold values from -0.125 to 0.125
- attn_gain: float32 [2048], replicated, may hold values from 0.1 to 1.9
- mlp_gain: float32 [2048], replicated, may hold values from 0.1 to 1.9
- gate_weight: bfloat16 [2048, 4096], P('sp', 'tp'), may hold values from -0.125 to 0.125
- up_weight: bfloat16 [2048, 4096], P('sp', 'tp'), may hold values from -0.125 to 0.125
- down_weight: bfloat16 [4096, 2048], P('tp', 'sp'), may hold values from -0.375 to 0.375
Outputs:
- mixed: bfloat16 [4096, 2048], P(('sp', 'tp'))
Inputs may be any that keep to these rules, and one draw needn't show every extreme that they name: `log_gates`: each head's row never rises from one position to the next and starts at or below 0. `documents`: document numbers never fall along the positions; one document spans exactly three quarters of the 4096 positions.
All inputs are finite; a program needn't handle non-finite values.
Results may differ from a plain program's by a relative error of at most 0.018.
Values may be sent and summed in bfloat16 or wider, within the bound.
A program may use at most 64 MiB of HBM per device.

v0:
```python
import math
import jax
import jax.numpy as jnp
from jax import lax
from jax.sharding import PartitionSpec as P

HD = 128


def local(
    resid,
    queries,
    keys,
    values,
    log_gates,
    documents,
    out_weight,
    attn_gain,
    mlp_gain,
    gate_weight,
    up_weight,
    down_weight,
):
    tok_rows = queries.shape[0]
    kv_dev = keys.shape[1] // HD
    heads_dev = log_gates.shape[0]
    group_size = heads_dev // kv_dev
    score_scale = 1.0 / math.sqrt(HD)
    own_start = lax.axis_index("sp") * tok_rows
    own_last = own_start + tok_rows - 1
    first_doc = documents[0]
    query_pos = own_start + lax.iota(jnp.int32, tok_rows)
    query_heads = queries.reshape(tok_rows, kv_dev, group_size, HD)
    key_gates_all = log_gates.reshape(kv_dev, group_size, log_gates.shape[1])
    query_gates = lax.dynamic_slice_in_dim(key_gates_all, own_start, tok_rows, 2)
    collected = (
        lax.all_gather(gate_weight, "sp", axis=0, tiled=True),
        lax.all_gather(up_weight, "sp", axis=0, tiled=True),
        lax.all_gather(down_weight, "sp", axis=1, tiled=True),
    )
    residual_rows = resid.astype(jnp.float32)

    def attend_block(running, key_rows, value_rows, doc_rows, first_row):
        run_max, run_sum, accumulated = running
        key_count = key_rows.shape[0]
        scores = (
            jnp.einsum(
                "tkgd,skd->kgts",
                query_heads,
                key_rows.reshape(key_count, kv_dev, HD),
                preferred_element_type=jnp.float32,
            )
            * score_scale
        )
        key_gates = lax.dynamic_slice_in_dim(key_gates_all, first_row, key_count, 2)
        scores = scores + query_gates[..., None] - key_gates[:, :, None, :]
        key_pos = first_row + lax.iota(jnp.int32, key_count)
        visible = (key_pos[None, :] <= query_pos[:, None]) & (
            doc_rows[None, :] == documents[:, None]
        )
        scores = jnp.where(visible, scores, jnp.float32(-1e30))
        new_max = jnp.maximum(run_max, jnp.max(scores, axis=-1))
        probs = jnp.where(visible, jnp.exp(scores - new_max[..., None]), jnp.float32(0.0))
        shrink = jnp.exp(run_max - new_max)
        run_sum = run_sum * shrink + jnp.sum(probs, axis=-1)
        weighted = jnp.einsum(
            "kgts,skd->kgtd",
            probs.astype(jnp.bfloat16),
            value_rows.reshape(key_count, kv_dev, HD),
            preferred_element_type=jnp.float32,
        )
        accumulated = accumulated * shrink[..., None] + weighted
        return (new_max, run_sum, accumulated)

    def maybe_attend(running, key_rows, value_rows, doc_rows, first_row):
        needed = (first_row <= own_last) & (doc_rows[-1] >= first_doc)

        def compute(state):
            return attend_block(state, key_rows, value_rows, doc_rows, first_row)

        def keep(state):
            return state

        return lax.cond(needed, compute, keep, running)

    start_state = (
        jnp.full((kv_dev, group_size, tok_rows), -1e30, jnp.float32),
        jnp.zeros((kv_dev, group_size, tok_rows), jnp.float32),
        jnp.zeros((kv_dev, group_size, tok_rows, HD), jnp.float32),
    )
    key_rows = lax.all_gather(keys, "sp", axis=0, tiled=True)
    value_rows = lax.all_gather(values, "sp", axis=0, tiled=True)
    doc_rows = lax.all_gather(documents, "sp", axis=0, tiled=True)
    key_count = key_rows.shape[0]
    block_len = math.gcd(key_count, 1024)

    def advance(block_index, inner):
        offset = block_index * block_len
        return maybe_attend(
            inner,
            lax.dynamic_slice_in_dim(key_rows, offset, block_len, 0),
            lax.dynamic_slice_in_dim(value_rows, offset, block_len, 0),
            lax.dynamic_slice_in_dim(doc_rows, offset, block_len, 0),
            offset,
        )

    run_max, run_sum, accumulated = lax.fori_loop(0, key_count // block_len, advance, start_state)
    attended = accumulated / run_sum[..., None]
    attended = (
        jnp.transpose(attended, (2, 0, 1, 3)).reshape(tok_rows, heads_dev * HD).astype(jnp.bfloat16)
    )
    rows_slice = attended
    projected = lax.psum_scatter(
        jnp.dot(rows_slice, out_weight, preferred_element_type=jnp.float32).astype(jnp.bfloat16),
        "tp",
        scatter_dimension=0,
        tiled=True,
    ).astype(jnp.float32)
    power = jnp.mean(projected * projected, axis=-1, keepdims=True)
    middle = residual_rows + attn_gain * projected * lax.rsqrt(power + 1e-06)
    middle_power = jnp.mean(middle * middle, axis=-1, keepdims=True)
    normed = (mlp_gain * middle * lax.rsqrt(middle_power + 1e-06)).astype(jnp.bfloat16)
    normed_all = lax.all_gather(normed, "tp", axis=0, tiled=True)
    gate_full, up_full, down_full = collected
    gate_act = jnp.dot(normed_all, gate_full, preferred_element_type=jnp.float32)
    up_act = jnp.dot(normed_all, up_full, preferred_element_type=jnp.float32)
    hidden = (jax.nn.silu(gate_act) * up_act).astype(jnp.bfloat16)
    rows_slice = hidden
    lowered = lax.psum_scatter(
        jnp.dot(rows_slice, down_full, preferred_element_type=jnp.float32).astype(jnp.bfloat16),
        "tp",
        scatter_dimension=0,
        tiled=True,
    ).astype(jnp.float32)
    return (middle + 0.5 * lowered).astype(jnp.bfloat16)


def solution(mesh):
    placed = (
        P(("sp", "tp"), None),
        P("sp", "tp"),
        P("sp", "tp"),
        P("sp", "tp"),
        P("tp", None),
        P("sp"),
        P("tp", None),
        P(),
        P(),
        P("sp", "tp"),
        P("sp", "tp"),
        P("tp", "sp"),
    )
    return jax.shard_map(
        local, mesh=mesh, in_specs=placed, out_specs=P(("sp", "tp"), None), check_vma=False
    )
```

profile of v0, /device:TPU:0, one launch (start us, length us, event | category | flops | bytes accessed | tf_op | source)
XLA Modules:
  0.0 661.0 jit_solution(3229841452047718858)
XLA Ops:
  6.5 1.8 copy.27
  8.3 0.0 all-gather.10.cloned.1.call-update
  8.4 0.0 all-gather.8.cloned.1.call-start
  8.4 1.8 copy.25
  10.2 0.0 all-gather.8.cloned.1.call-update
  10.2 0.0 reduce-scatter.3.cloned.1.call-start
  10.3 1.0 reshape.49
  11.3 1.2 copy.26
  12.5 0.3 copy.28
  12.8 1.2 slice.10
  14.0 43.0 %all-gather = s32[16,1,256]{2,1,0:T(1,128)S(1)} all-gather(s32[1,1,256]{2,1,0:T(1,128)} %bitcast.62), channel_id=1, replica_groups=mesh['sp'=16,'tp'=2] {'sp'}, dimensions={0}, use_global_device_ids=true | all-gather | bytes 17408 | tf_op jit(solution)/shard_map/all_gather | solution.py:93
  56.9 42.7 %all-gather.10.cloned.1.call-done = bf16[4096,512]{0,1:T(8,128)(2,1)} async-done(((bf16[256,512]{0,1:T(8,128)(2,1)}), bf16[4096,512]{0,1:T(8,128)(2,1)}) %all-gather.10.cloned.1.call-update) | async-done | bytes 4194320 | tf_op jit(solution)/shard_map/all_gather | solution.py:92
  99.7 87.7 %all-gather.8.cloned.1.call-done = bf16[4096,512]{0,1:T(8,128)(2,1)} async-done(((bf16[256,512]{0,1:T(8,128)(2,1)}), bf16[4096,512]{0,1:T(8,128)(2,1)}) %all-gather.8.cloned.1.call-update) | async-done | bytes 4194320 | tf_op jit(solution)/shard_map/all_gather | solution.py:91
  187.4 0.1 broadcast_in_dim.42
  187.5 20.5 %while.18 = (s32[]{:T(128)}, f32[4,2,256]{2,1,0:T(2,128)S(1)}, f32[4,2,256]{2,1,0:T(2,128)S(1)}, f32[4,2,256,128]{3,2,1,0:T(8,128)S(1)}, s32[]{:T(128)}, /*index...) while((s32[]{:T(128)}, f32[4,2,256]{2,1,0:T(2,128)S(1)}, ...), condition=%wide.region_5.6_spmd.clone, body=%wide.region_0.5_spmd.clone.sunk | while | flops 1114903808 | bytes 35472848 | solution.py:107
  187.5 0.6 slice.13
  189.3 13.1 %conditional.3 = ((f32[4,2,256]{2,1,0:T(2,128)S(1)}, f32[4,2,256]{2,1,0:T(2,128)S(1)}, f32[4,2,256,128]{3,2,1,0:T(8,128)S(1)})) conditional(s32[]{:T(128)} %convert_element_type.92, (f32[4,2,256]{2,1,0:T(2,128)S(1)}, f32[4,2,256]{2,1,0:T(2,128)S(1)}, f32[4,2,256,128]{3,2,1,0:T(8,128)S(1)}) %tuple.52, (s32[]{:T(128)}, s32[]{:T(128)}, ...), branch_computations={%region_1.0_spmd, %region_2.4_spmd} | conditional | flops 1114903808 | bytes 35463248 | solution.py:84
  189.4 1.0 compare_and_fusion
  190.4 1.7 constant_dynamic-slice_fusion
  192.2 3.0 fusion.6
  195.2 3.0 fusion.5
  198.3 4.1 fusion.10
  202.5 0.6 slice.13
  204.3 0.6 slice.13
  206.2 0.6 slice.13
  208.1 0.3 copy.29
  208.4 0.1 divide_convert_fusion
  208.5 4.4 convolution_convert_fusion
  213.0 0.0 all-gather.12.cloned.1.call-start
  213.0 32.8 %reduce-scatter.3.cloned.1.call-done = bf16[128,2048]{1,0:T(8,128)(2,1)} async-done(((bf16[256,2048]{1,0:T(8,128)(2,1)}), bf16[128,2048]{1,0:T(8,128)(2,1)}) %reduce-scatter.3.cloned.1.call-update) | async-done | bytes 524304 | tf_op jit(solution)/shard_map/reduce_scatter | solution.py:113
  245.8 1.2 fusion.19
  247.1 1.4 multiply_reduce_fusion
  248.5 2.2 multiply_convert_fusion
  250.8 0.0 all-gather.14.cloned.1.call-start
  250.8 0.5 all-gather.14.cloned.1.call-update
  251.4 0.0 all-gather.16.cloned.1.call-start
  251.4 0.5 all-gather.16.cloned.1.call-update
  251.9 0.0 all-gather.18.cloned.1.call-start
  252.0 0.7 all-gather.18.cloned.1.call-update
  252.7 0.2 reduce-scatter.5.cloned.1.call-start
  252.9 8.2 %all-gather.12.cloned.1.call-done = bf16[256,2048]{1,0:T(8,128)(2,1)} async-done(((bf16[128,2048]{1,0:T(8,128)(2,1)}), bf16[256,2048]{1,0:T(8,128)(2,1)}) %all-gather.12.cloned.1.call-update) | async-done | bytes 1048592 | tf_op jit(solution)/shard_map/all_gather | solution.py:123
  261.2 116.1 %all-gather.14.cloned.1.call-done = bf16[2048,2048]{1,0:T(8,128)(2,1)} async-done(((bf16[128,2048]{1,0:T(8,128)(2,1)}), bf16[2048,2048]{1,0:T(8,128)(2,1)}) %all-gather.14.cloned.1.call-update) | async-done | bytes 8388624 | tf_op jit(solution)/shard_map/all_gather | solution.py:37
  377.3 7.4 %fusion.21 = f32[256,2048]{1,0:T(8,128)} fusion(bf16[256,2048]{1,0:T(8,128)(2,1)} %all-gather.12.cloned.1.call-done, bf16[2048,2048]{1,0:T(8,128)(2,1)} %all-gather.14.cloned.1.call-done), kind=kOutput, calls=%fused_computation.39 | convolution fusion | flops 2147483648 | bytes 11534336 | tf_op jit(solution)/shard_map/dot_general | solution.py:125
  384.7 105.7 %all-gather.16.cloned.1.call-done = bf16[2048,2048]{1,0:T(8,128)(2,1)} async-done(((bf16[128,2048]{1,0:T(8,128)(2,1)}), bf16[2048,2048]{1,0:T(8,128)(2,1)}) %all-gather.16.cloned.1.call-update) | async-done | bytes 8388624 | tf_op jit(solution)/shard_map/all_gather | solution.py:38
  490.4 142.7 %all-gather.18.cloned.1.call-done = bf16[2048,2048]{1,0:T(8,128)(2,1)} async-done(((bf16[2048,128]{1,0:T(8,128)(2,1)}), bf16[2048,2048]{1,0:T(8,128)(2,1)}) %all-gather.18.cloned.1.call-update) | async-done | bytes 8388624 | tf_op jit(solution)/shard_map/all_gather | solution.py:39
  633.1 12.1 %convolution_convert_fusion.1 = bf16[256,2048]{1,0:T(8,128)(2,1)} fusion(bf16[2048,2048]{1,0:T(8,128)(2,1)} %all-gather.18.cloned.1.call-done, bf16[256,2048]{1,0:T(8,128)(2,1)S(1)} %copy-done.4, bf16[2048,2048]{1,0:T(8,128)(2,1)} %all-gather.16.cloned.1.call-done, f32[256,2048]{1,0:T(8,128)} %fusion.21), kind=kOutput, calls=%fused_computation.25 | convolution fusion | flops 4298637312 | bytes 20971520 | tf_op jit(solution)/shard_map/dot_general | solution.py:130
  645.3 6.7 %reduce-scatter.5.cloned.1.call-done = bf16[128,2048]{1,0:T(8,128)(2,1)} async-done(((bf16[256,2048]{1,0:T(8,128)(2,1)}), bf16[128,2048]{1,0:T(8,128)(2,1)}) %reduce-scatter.5.cloned.1.call-update) | async-done | bytes 524304 | tf_op jit(solution)/shard_map/reduce_scatter | solution.py:129
  652.0 2.2 add_convert_fusion
  (36 shorter events, 0.2 us)
Async XLA Ops:
  6.5 93.2 %all-gather.10.cloned.1.call-start = ((), (), s32[]{:S(2)}) async-start(), calls=%async_computation.3 | async-start | bytes 4456448 | tf_op jit(solution)/shard_map/all_gather | solution.py:92
  8.4 179.0 %all-gather.8.cloned.1.call-start = ((), (), s32[]{:S(2)}) async-start(), calls=%async_computation.2 | async-start | bytes 4456448 | tf_op jit(solution)/shard_map/all_gather | solution.py:91
  10.2 235.6 %reduce-scatter.3.cloned.1.call-start = ((), (), s32[]{:S(2)}) async-start(), calls=%async_computation.4 | async-start | bytes 1572864 | tf_op jit(solution)/shard_map/reduce_scatter | solution.py:113
  208.0 39.0 %copy-start.1 = (bf16[128,2048]{1,0:T(8,128)(2,1)S(1)}, bf16[128,2048]{1,0:T(8,128)(2,1)}, u32[]{:S(2)}) copy-start(bf16[128,2048]{1,0:T(8,128)(2,1)} %param.16) | copy-start | bytes 1572868
  208.0 39.0 %copy-start.2 = (f32[2048]{0:T(1024)S(1)}, f32[2048]{0:T(1024)}, u32[]{:S(2)}) copy-start(f32[2048]{0:T(1024)} %param.23) | copy-start | bytes 24580
  208.1 40.5 %copy-start.3 = (f32[2048]{0:T(1024)S(1)}, f32[2048]{0:T(1024)}, u32[]{:S(2)}) copy-start(f32[2048]{0:T(1024)} %param.24) | copy-start | bytes 24580
  213.0 48.2 %all-gather.12.cloned.1.call-start = ((), (), s32[]{:S(2)}) async-start(), calls=%async_computation.5 | async-start | bytes 1572864 | tf_op jit(solution)/shard_map/all_gather | solution.py:123
  250.8 126.5 %all-gather.14.cloned.1.call-start = ((), (), s32[]{:S(2)}) async-start(), calls=%async_computation.6 | async-start | bytes 8912896 | tf_op jit(solution)/shard_map/all_gather | solution.py:37
  251.4 239.1 %all-gather.16.cloned.1.call-start = ((), (), s32[]{:S(2)}) async-start(), calls=%async_computation.7 | async-start | bytes 8912896 | tf_op jit(solution)/shard_map/all_gather | solution.py:38
  251.9 381.2 %all-gather.18.cloned.1.call-start = ((), (), s32[]{:S(2)}) async-start(), calls=%async_computation.8 | async-start | bytes 8912896 | tf_op jit(solution)/shard_map/all_gather | solution.py:39
  252.7 399.4 %reduce-scatter.5.cloned.1.call-start = ((), (), s32[]{:S(2)}) async-start(), calls=%async_computation.9 | async-start | bytes 1572864 | tf_op jit(solution)/shard_map/reduce_scatter | solution.py:129
  261.2 372.0 %copy-start.4 = (bf16[256,2048]{1,0:T(8,128)(2,1)S(1)}, bf16[256,2048]{1,0:T(8,128)(2,1)}, u32[]{:S(2)}) copy-start(bf16[256,2048]{1,0:T(8,128)(2,1)} %all-gather.12.cloned.1.call-done) | copy-start | bytes 3145732
  384.7 267.3 %copy-start = (bf16[128,2048]{1,0:T(8,128)(2,1)S(1)}, bf16[128,2048]{1,0:T(8,128)(2,1)}, u32[]{:S(2)}) copy-start(bf16[128,2048]{1,0:T(8,128)(2,1)} %reduce-scatter.3.cloned.1.call-done) | copy-start | bytes 1572868
Sparse Core Ops, SparseCore 0:
  10.1 89.5 all-gather.9
  102.4 84.9 all-gather.7
  213.1 32.6 reduce-scatter.2
  250.9 10.2 all-gather.11
  263.8 113.4 all-gather.13
  379.9 110.4 all-gather.15
  493.1 139.9 all-gather.17
  645.4 6.5 reduce-scatter.4
where the time goes:
time: 662 us; the launch traced here: 661 us
  waiting for transfers between devices  545 us (82%)
  blocking collectives  43 us (6%)
  matrix products  31.2 us (5%)
  between operations  13.6 us (2%)
  local copies, waits for them, and re-layouts  11.9 us (2%)
  other arithmetic  11.2 us (2%)
    all_gather x1, waiting for transfers between devices, local(): lax.all_gather(down_weight, 'sp', axis=1, tiled=True)  143 us
    all_gather x1, waiting for transfers between devices, local(): lax.all_gather(gate_weight, 'sp', axis=0, tiled=True)  116 us
    all_gather x1, waiting for transfers between devices, local(): lax.all_gather(up_weight, 'sp', axis=0, tiled=True)  106 us
    all_gather x1, waiting for transfers between devices, local(): key_rows = lax.all_gather(keys, 'sp', axis=0, tiled=True)  87.7 us
    all_gather x1, blocking collectives, local(): doc_rows = lax.all_gather(documents, 'sp', axis=0, tiled=True)  43 us
    all_gather x1, waiting for transfers between devices, local(): value_rows = lax.all_gather(values, 'sp', axis=0, tiled=True)  42.7 us
    reduce_scatter x1, waiting for transfers between devices, local(): lax.psum_scatter(jnp.dot(rows_slice, out_weight, preferred_element_type=j...  32.8 us
  transfers between devices with their start and end apart: 8, of which 8 were waited for; matrix products, arithmetic and copies ran while one was open for 2% of the time, Pallas kernels for 0%

commit v1 on v0

--- a/solution.py
+++ b/solution.py
@@ -88,7 +88,12 @@
         jnp.zeros((kv_dev, group_size, tok_rows), jnp.float32),
         jnp.zeros((kv_dev, group_size, tok_rows, HD), jnp.float32),
     )
-    key_rows = lax.all_gather(keys, "sp", axis=0, tiled=True)
+    ring = [keys]
+    for hop in range(15):
+        ring.append(lax.ppermute(ring[-1], "sp", [(dev, (dev + 1) % 16) for dev in range(16)]))
+    key_rows = jnp.roll(
+        jnp.concatenate(ring[::-1], axis=0), (lax.axis_index("sp") + 1) * ring[0].shape[0], axis=0
+    )
     value_rows = lax.all_gather(values, "sp", axis=0, tiled=True)
     doc_rows = lax.all_gather(documents, "sp", axis=0, tiled=True)
     key_count = key_rows.shape[0]

time: 662 us -> 716 us (1.082)
  waiting for transfers between devices: 545 us -> 579 us
  local copies, waits for them, and re-layouts: 11.9 us -> 26.9 us
    ppermute x0 -> x15, waiting for transfers between devices: none -> 173 us  [local(): lax.ppermute(ring[-1], 'sp', [(dev, (dev + 1) % 16) for dev in range(16)])]
    all_gather x1 -> x0, waiting for transfers between devices: 87.7 us -> none  [local(): key_rows = lax.all_gather(keys, 'sp', axis=0, tiled=True)]
    all_gather x1, waiting for transfers between devices: 42.7 us -> 0.01 us  [local(): value_rows = lax.all_gather(values, 'sp', axis=0, tiled=True)]
    unnamed x14 -> x59, local copies, waits for them, and re-layouts: 5.14 us -> 14.8 us
    reduce_scatter x1, waiting for transfers between devices: 32.8 us -> 24.9 us  [local(): lax.psum_scatter(jnp.dot(rows_slice, out_weight, preferred_element_type=j...]
  transfers between devices with their start and end apart: 8 -> 22, of which waited for: 8 -> 20; matrix products, arithmetic and copies ran while one was open for 2% -> 3% of each run, Pallas kernels for 0% -> 0%
where the time goes in v1:
time: 716 us; the launch traced here: 715 us
  waiting for transfers between devices  579 us (81%)
  blocking collectives  43.2 us (6%)
  matrix products  32.2 us (4%)
  local copies, waits for them, and re-layouts  26.9 us (4%)
  between operations  13.9 us (2%)
  other arithmetic  10.6 us (1%)
    ppermute x15, waiting for transfers between devices, local(): lax.ppermute(ring[-1], 'sp', [(dev, (dev + 1) % 16) for dev in range(16)])  173 us
    all_gather x1, waiting for transfers between devices, local(): lax.all_gather(down_weight, 'sp', axis=1, tiled=True)  143 us
    all_gather x1, waiting for transfers between devices, local(): lax.all_gather(gate_weight, 'sp', axis=0, tiled=True)  116 us
    all_gather x1, waiting for transfers between devices, local(): lax.all_gather(up_weight, 'sp', axis=0, tiled=True)  106 us
    all_gather x1, blocking collectives, local(): doc_rows = lax.all_gather(documents, 'sp', axis=0, tiled=True)  43.2 us
    reduce_scatter x1, waiting for transfers between devices, local(): lax.psum_scatter(jnp.dot(rows_slice, out_weight, preferred_element_type=j...  24.9 us
    unnamed x59, local copies, waits for them, and re-layouts  14.8 us
  transfers between devices with their start and end apart: 22, of which 20 were waited for; matrix products, arithmetic and copies ran while one was open for 3% of the time, Pallas kernels for 0%

profile of v1, /device:TPU:0, one launch (start us, length us, event | category | flops | bytes accessed | tf_op | source)
XLA Modules:
  0.0 715.0 jit_solution(18133810573093827618)
XLA Ops:
  6.5 1.1 copy.27
  7.6 3.0 collective-permute-start
  10.6 10.3 %collective-permute-done = bf16[256,512]{0,1:T(8,128)(2,1)S(1)} collective-permute-done((bf16[256,512]{0,1:T(8,128)(2,1)S(1)}, bf16[256,512]{0,1:T(8,128)(2,1)S(1)}, u32[]{:S(2)}, u32[]{:S(2)}) %collective-permute-start) | collective-permute-done | bytes 262176 | tf_op jit(solution)/shard_map/ppermute | solution.py:93
  20.9 1.8 copy.31
  22.8 9.2 %collective-permute-done.1 = bf16[256,512]{0,1:T(8,128)(2,1)S(1)} collective-permute-done((bf16[256,512]{0,1:T(8,128)(2,1)S(1)}, bf16[256,512]{0,1:T(8,128)(2,1)S(1)}, u32[]{:S(2)}, u32[]{:S(2)}) %collective-permute-start.1) | collective-permute-done | bytes 262176 | tf_op jit(solution)/shard_map/ppermute | solution.py:93
  32.0 11.8 %collective-permute-done.2 = bf16[256,512]{0,1:T(8,128)(2,1)S(1)} collective-permute-done((bf16[256,512]{0,1:T(8,128)(2,1)S(1)}, bf16[256,512]{0,1:T(8,128)(2,1)S(1)}, u32[]{:S(2)}, u32[]{:S(2)}) %collective-permute-start.2) | collective-permute-done | bytes 262176 | tf_op jit(solution)/shard_map/ppermute | solution.py:93
  43.8 10.0 %collective-permute-done.3 = bf16[256,512]{0,1:T(8,128)(2,1)S(1)} collective-permute-done((bf16[256,512]{0,1:T(8,128)(2,1)S(1)}, bf16[256,512]{0,1:T(8,128)(2,1)S(1)}, u32[]{:S(2)}, u32[]{:S(2)}) %collective-permute-start.3) | collective-permute-done | bytes 262176 | tf_op jit(solution)/shard_map/ppermute | solution.py:93
  53.8 14.1 %collective-permute-done.4 = bf16[256,512]{0,1:T(8,128)(2,1)S(1)} collective-permute-done((bf16[256,512]{0,1:T(8,128)(2,1)S(1)}, bf16[256,512]{0,1:T(8,128)(2,1)S(1)}, u32[]{:S(2)}, u32[]{:S(2)}) %collective-permute-start.4) | collective-permute-done | bytes 262176 | tf_op jit(solution)/shard_map/ppermute | solution.py:93
  67.9 14.1 %collective-permute-done.5 = bf16[256,512]{0,1:T(8,128)(2,1)S(1)} collective-permute-done((bf16[256,512]{0,1:T(8,128)(2,1)S(1)}, bf16[256,512]{0,1:T(8,128)(2,1)S(1)}, u32[]{:S(2)}, u32[]{:S(2)}) %collective-permute-start.5) | collective-permute-done | bytes 262176 | tf_op jit(solution)/shard_map/ppermute | solution.py:93
  82.0 18.1 %collective-permute-done.6 = bf16[256,512]{0,1:T(8,128)(2,1)S(1)} collective-permute-done((bf16[256,512]{0,1:T(8,128)(2,1)S(1)}, bf16[256,512]{0,1:T(8,128)(2,1)S(1)}, u32[]{:S(2)}, u32[]{:S(2)}) %collective-permute-start.6) | collective-permute-done | bytes 262176 | tf_op jit(solution)/shard_map/ppermute | solution.py:93
  100.1 18.0 %collective-permute-done.7 = bf16[256,512]{0,1:T(8,128)(2,1)S(1)} collective-permute-done((bf16[256,512]{0,1:T(8,128)(2,1)S(1)}, bf16[256,512]{0,1:T(8,128)(2,1)S(1)}, u32[]{:S(2)}, u32[]{:S(2)}) %collective-permute-start.7) | collective-permute-done | bytes 262176 | tf_op jit(solution)/shard_map/ppermute | solution.py:93
  118.1 17.7 %collective-permute-done.8 = bf16[256,512]{0,1:T(8,128)(2,1)S(1)} collective-permute-done((bf16[256,512]{0,1:T(8,128)(2,1)S(1)}, bf16[256,512]{0,1:T(8,128)(2,1)S(1)}, u32[]{:S(2)}, u32[]{:S(2)}) %collective-permute-start.8) | collective-permute-done | bytes 262176 | tf_op jit(solution)/shard_map/ppermute | solution.py:93
  135.8 10.0 %collective-permute-done.9 = bf16[256,512]{0,1:T(8,128)(2,1)S(1)} collective-permute-done((bf16[256,512]{0,1:T(8,128)(2,1)S(1)}, bf16[256,512]{0,1:T(8,128)(2,1)S(1)}, u32[]{:S(2)}, u32[]{:S(2)}) %collective-permute-start.9) | collective-permute-done | bytes 262176 | tf_op jit(solution)/shard_map/ppermute | solution.py:93
  145.7 10.0 %collective-permute-done.10 = bf16[256,512]{0,1:T(8,128)(2,1)S(1)} collective-permute-done((bf16[256,512]{0,1:T(8,128)(2,1)S(1)}, bf16[256,512]{0,1:T(8,128)(2,1)S(1)}, u32[]{:S(2)}, u32[]{:S(2)}) %collective-permute-start.10) | collective-permute-done | bytes 262176 | tf_op jit(solution)/shard_map/ppermute | solution.py:93
  156.4 10.0 %collective-permute-done.11 = bf16[256,512]{0,1:T(8,128)(2,1)S(1)} collective-permute-done((bf16[256,512]{0,1:T(8,128)(2,1)S(1)}, bf16[256,512]{0,1:T(8,128)(2,1)S(1)}, u32[]{:S(2)}, u32[]{:S(2)}) %collective-permute-start.11) | collective-permute-done | bytes 262176 | tf_op jit(solution)/shard_map/ppermute | solution.py:93
  167.1 10.0 %collective-permute-done.12 = bf16[256,512]{0,1:T(8,128)(2,1)S(1)} collective-permute-done((bf16[256,512]{0,1:T(8,128)(2,1)S(1)}, bf16[256,512]{0,1:T(8,128)(2,1)S(1)}, u32[]{:S(2)}, u32[]{:S(2)}) %collective-permute-start.12) | collective-permute-done | bytes 262176 | tf_op jit(solution)/shard_map/ppermute | solution.py:93
  177.8 10.1 %collective-permute-done.13 = bf16[256,512]{0,1:T(8,128)(2,1)} collective-permute-done((bf16[256,512]{0,1:T(8,128)(2,1)S(1)}, bf16[256,512]{0,1:T(8,128)(2,1)}, u32[]{:S(2)}, u32[]{:S(2)}) %collective-permute-start.13) | collective-permute-done | bytes 262176 | tf_op jit(solution)/shard_map/ppermute | solution.py:93
  187.9 1.0 reshape.49
  188.8 1.2 copy.30
  190.1 1.0 copy.32
  191.1 1.3 slice.10
  192.4 43.2 %all-gather = s32[16,1,256]{2,1,0:T(1,128)} all-gather(s32[1,1,256]{2,1,0:T(1,128)} %bitcast.62), channel_id=1, replica_groups=mesh['sp'=16,'tp'=2] {'sp'}, dimensions={0}, use_global_device_ids=true | all-gather | bytes 17408 | tf_op jit(solution)/shard_map/all_gather | solution.py:98
  236.6 1.0 constant_dynamic-update-slice_fusion.30
  237.6 1.0 constant_dynamic-update-slice_fusion.29
  238.5 1.0 constant_dynamic-update-slice_fusion.28
  239.5 1.0 constant_dynamic-update-slice_fusion.27
  240.9 1.0 constant_dynamic-update-slice_fusion.15
  241.9 1.0 constant_dynamic-update-slice_fusion.14
  243.4 2.3 constant_dynamic-slice_fusion.4
  245.8 24.2 %while.18 = (s32[]{:T(128)}, f32[4,2,256]{2,1,0:T(2,128)S(1)}, f32[4,2,256]{2,1,0:T(2,128)S(1)}, f32[4,2,256,128]{3,2,1,0:T(8,128)S(1)}, s32[]{:T(128)}, /*index...) while((s32[]{:T(128)}, f32[4,2,256]{2,1,0:T(2,128)S(1)}, ...), condition=%wide.region_5.6_spmd.clone, body=%wide.region_0.5_spmd.clone.sunk | while | flops 1114903808 | bytes 35472848 | solution.py:112
  248.5 13.4 %conditional.3 = ((f32[4,2,256]{2,1,0:T(2,128)S(1)}, f32[4,2,256]{2,1,0:T(2,128)S(1)}, f32[4,2,256,128]{3,2,1,0:T(8,128)S(1)})) conditional(s32[]{:T(128)} %convert_element_type.92, (f32[4,2,256]{2,1,0:T(2,128)S(1)}, f32[4,2,256]{2,1,0:T(2,128)S(1)}, f32[4,2,256,128]{3,2,1,0:T(8,128)S(1)}) %tuple.52, (s32[]{:T(128)}, s32[]{:T(128)}, ...), branch_computations={%region_1.1_spmd, %region_2.4_spmd} | conditional | flops 1114903808 | bytes 35463248 | solution.py:84
  248.9 1.7 constant_dynamic-slice_fusion
  250.7 4.1 fusion.6
  254.7 3.0 fusion.5
  257.8 4.1 fusion.10
  270.6 4.4 convolution_convert_fusion
  275.1 24.9 %reduce-scatter.3.cloned.1.call-done = bf16[128,2048]{1,0:T(8,128)(2,1)} async-done(((bf16[256,2048]{1,0:T(8,128)(2,1)}), bf16[128,2048]{1,0:T(8,128)(2,1)}) %reduce-scatter.3.cloned.1.call-update) | async-done | bytes 524304 | tf_op jit(solution)/shard_map/reduce_scatter | solution.py:118
  299.9 1.2 fusion.19
  301.2 1.4 multiply_reduce_fusion
  302.6 2.2 multiply_convert_fusion
  306.9 8.4 %all-gather.9.cloned.1.call-done = bf16[256,2048]{1,0:T(8,128)(2,1)} async-done(((bf16[128,2048]{1,0:T(8,128)(2,1)}), bf16[256,2048]{1,0:T(8,128)(2,1)}) %all-gather.9.cloned.1.call-update) | async-done | bytes 1048592 | tf_op jit(solution)/shard_map/all_gather | solution.py:128
  315.3 116.1 %all-gather.11.cloned.1.call-done = bf16[2048,2048]{1,0:T(8,128)(2,1)} async-done(((bf16[128,2048]{1,0:T(8,128)(2,1)}), bf16[2048,2048]{1,0:T(8,128)(2,1)}) %all-gather.11.cloned.1.call-update) | async-done | bytes 8388624 | tf_op jit(solution)/shard_map/all_gather | solution.py:37
  431.4 7.4 %fusion.21 = f32[256,2048]{1,0:T(8,128)} fusion(bf16[256,2048]{1,0:T(8,128)(2,1)} %all-gather.9.cloned.1.call-done, bf16[2048,2048]{1,0:T(8,128)(2,1)} %all-gather.11.cloned.1.call-done), kind=kOutput, calls=%fused_computation.72 | convolution fusion | flops 2147483648 | bytes 11534336 | tf_op jit(solution)/shard_map/dot_general | solution.py:130
  438.8 105.7 %all-gather.13.cloned.1.call-done = bf16[2048,2048]{1,0:T(8,128)(2,1)} async-done(((bf16[128,2048]{1,0:T(8,128)(2,1)}), bf16[2048,2048]{1,0:T(8,128)(2,1)}) %all-gather.13.cloned.1.call-update) | async-done | bytes 8388624 | tf_op jit(solution)/shard_map/all_gather | solution.py:38
  544.5 142.6 %all-gather.15.cloned.1.call-done = bf16[2048,2048]{1,0:T(8,128)(2,1)} async-done(((bf16[2048,128]{1,0:T(8,128)(2,1)}), bf16[2048,2048]{1,0:T(8,128)(2,1)}) %all-gather.15.cloned.1.call-update) | async-done | bytes 8388624 | tf_op jit(solution)/shard_map/all_gather | solution.py:39
  687.1 12.1 %convolution_convert_fusion.1 = bf16[256,2048]{1,0:T(8,128)(2,1)} fusion(bf16[2048,2048]{1,0:T(8,128)(2,1)} %all-gather.15.cloned.1.call-done, bf16[256,2048]{1,0:T(8,128)(2,1)S(1)} %copy-done.11, bf16[2048,2048]{1,0:T(8,128)(2,1)} %all-gather.13.cloned.1.call-done, f32[256,2048]{1,0:T(8,128)} %fusion.21), kind=kOutput, calls=%fused_computation.25 | convolution fusion | flops 4298637312 | bytes 20971520 | tf_op jit(solution)/shard_map/dot_general | solution.py:135
  699.3 6.7 reduce-scatter.5.cloned.1.call-done
  706.0 2.2 add_convert_fusion
  (110 shorter events, 12.3 us)
Async XLA Ops:
  6.5 239.2 %all-gather.7.cloned.1.call-start = ((), (), s32[]{:S(2)}) async-start(), calls=%async_computation.2 | async-start | bytes 4456448 | tf_op jit(solution)/shard_map/all_gather | solution.py:97
  7.6 13.3 %collective-permute-start = (bf16[256,512]{0,1:T(8,128)(2,1)S(1)}, bf16[256,512]{0,1:T(8,128)(2,1)S(1)}, u32[]{:S(2)}, u32[]{:S(2)}) collective-permute-start(bf16[256,512]{0,1:T(8,128)(2,1)S(1)} %copy.27), channel_id=1, source_target_pairs={{0,2},{2,4},{4,6},{6,8},{8,10},{10,12},{12,14},{14,16},{16,18},{18... | collective-permute-start | bytes 786440 | tf_op jit(solution)/shard_map/ppermute | solution.py:93
  20.9 11.1 %collective-permute-start.1 = (bf16[256,512]{0,1:T(8,128)(2,1)S(1)}, bf16[256,512]{0,1:T(8,128)(2,1)S(1)}, u32[]{:S(2)}, u32[]{:S(2)}) collective-permute-start(bf16[256,512]{0,1:T(8,128)(2,1)S(1)} %collective-permute-done), channel_id=1, source_target_pairs={{0,2},{2,4},{4,6},{6,8},{8,10},{10,12},{12,14},{14,16},{16,18},{18... | collective-permute-start | bytes 786440 | tf_op jit(solution)/shard_map/ppermute | solution.py:93
  22.8 277.2 %reduce-scatter.3.cloned.1.call-start = ((), (), s32[]{:S(2)}) async-start(), calls=%async_computation.3 | async-start | bytes 1572864 | tf_op jit(solution)/shard_map/reduce_scatter | solution.py:118
  32.0 11.8 %collective-permute-start.2 = (bf16[256,512]{0,1:T(8,128)(2,1)S(1)}, bf16[256,512]{0,1:T(8,128)(2,1)S(1)}, u32[]{:S(2)}, u32[]{:S(2)}) collective-permute-start(bf16[256,512]{0,1:T(8,128)(2,1)S(1)} %collective-permute-done.1), channel_id=1, source_target_pairs={{0,2},{2,4},{4,6},{6,8},{8,10},{10,12},{12,14},{14,16},{16,18},{18... | collective-permute-start | bytes 786440 | tf_op jit(solution)/shard_map/ppermute | solution.py:93
  43.8 10.0 %collective-permute-start.3 = (bf16[256,512]{0,1:T(8,128)(2,1)S(1)}, bf16[256,512]{0,1:T(8,128)(2,1)S(1)}, u32[]{:S(2)}, u32[]{:S(2)}) collective-permute-start(bf16[256,512]{0,1:T(8,128)(2,1)S(1)} %collective-permute-done.2), channel_id=1, source_target_pairs={{0,2},{2,4},{4,6},{6,8},{8,10},{10,12},{12,14},{14,16},{16,18},{18... | collective-permute-start | bytes 786440 | tf_op jit(solution)/shard_map/ppermute | solution.py:93
  53.8 14.1 %collective-permute-start.4 = (bf16[256,512]{0,1:T(8,128)(2,1)S(1)}, bf16[256,512]{0,1:T(8,128)(2,1)S(1)}, u32[]{:S(2)}, u32[]{:S(2)}) collective-permute-start(bf16[256,512]{0,1:T(8,128)(2,1)S(1)} %collective-permute-done.3), channel_id=1, source_target_pairs={{0,2},{2,4},{4,6},{6,8},{8,10},{10,12},{12,14},{14,16},{16,18},{18... | collective-permute-start | bytes 786440 | tf_op jit(solution)/shard_map/ppermute | solution.py:93
  67.9 14.1 %collective-permute-start.5 = (bf16[256,512]{0,1:T(8,128)(2,1)S(1)}, bf16[256,512]{0,1:T(8,128)(2,1)S(1)}, u32[]{:S(2)}, u32[]{:S(2)}) collective-permute-start(bf16[256,512]{0,1:T(8,128)(2,1)S(1)} %collective-permute-done.4), channel_id=1, source_target_pairs={{0,2},{2,4},{4,6},{6,8},{8,10},{10,12},{12,14},{14,16},{16,18},{18... | collective-permute-start | bytes 786440 | tf_op jit(solution)/shard_map/ppermute | solution.py:93
  82.0 18.1 %collective-permute-start.6 = (bf16[256,512]{0,1:T(8,128)(2,1)S(1)}, bf16[256,512]{0,1:T(8,128)(2,1)S(1)}, u32[]{:S(2)}, u32[]{:S(2)}) collective-permute-start(bf16[256,512]{0,1:T(8,128)(2,1)S(1)} %collective-permute-done.5), channel_id=1, source_target_pairs={{0,2},{2,4},{4,6},{6,8},{8,10},{10,12},{12,14},{14,16},{16,18},{18... | collective-permute-start | bytes 786440 | tf_op jit(solution)/shard_map/ppermute | solution.py:93
  100.1 18.0 %collective-permute-start.7 = (bf16[256,512]{0,1:T(8,128)(2,1)S(1)}, bf16[256,512]{0,1:T(8,128)(2,1)S(1)}, u32[]{:S(2)}, u32[]{:S(2)}) collective-permute-start(bf16[256,512]{0,1:T(8,128)(2,1)S(1)} %collective-permute-done.6), channel_id=1, source_target_pairs={{0,2},{2,4},{4,6},{6,8},{8,10},{10,12},{12,14},{14,16},{16,18},{18... | collective-permute-start | bytes 786440 | tf_op jit(solution)/shard_map/ppermute | solution.py:93
  118.1 17.7 %collective-permute-start.8 = (bf16[256,512]{0,1:T(8,128)(2,1)S(1)}, bf16[256,512]{0,1:T(8,128)(2,1)S(1)}, u32[]{:S(2)}, u32[]{:S(2)}) collective-permute-start(bf16[256,512]{0,1:T(8,128)(2,1)S(1)} %collective-permute-done.7), channel_id=1, source_target_pairs={{0,2},{2,4},{4,6},{6,8},{8,10},{10,12},{12,14},{14,16},{16,18},{18... | collective-permute-start | bytes 786440 | tf_op jit(solution)/shard_map/ppermute | solution.py:93
  135.8 10.0 %collective-permute-start.9 = (bf16[256,512]{0,1:T(8,128)(2,1)S(1)}, bf16[256,512]{0,1:T(8,128)(2,1)S(1)}, u32[]{:S(2)}, u32[]{:S(2)}) collective-permute-start(bf16[256,512]{0,1:T(8,128)(2,1)S(1)} %collective-permute-done.8), channel_id=1, source_target_pairs={{0,2},{2,4},{4,6},{6,8},{8,10},{10,12},{12,14},{14,16},{16,18},{18... | collective-permute-start | bytes 786440 | tf_op jit(solution)/shard_map/ppermute | solution.py:93
  145.7 10.0 %collective-permute-start.10 = (bf16[256,512]{0,1:T(8,128)(2,1)S(1)}, bf16[256,512]{0,1:T(8,128)(2,1)S(1)}, u32[]{:S(2)}, u32[]{:S(2)}) collective-permute-start(bf16[256,512]{0,1:T(8,128)(2,1)S(1)} %collective-permute-done.9), channel_id=1, source_target_pairs={{0,2},{2,4},{4,6},{6,8},{8,10},{10,12},{12,14},{14,16},{16,18},{18... | collective-permute-start | bytes 786440 | tf_op jit(solution)/shard_map/ppermute | solution.py:93
  155.7 0.7 copy-start.2
  156.4 10.0 %collective-permute-start.11 = (bf16[256,512]{0,1:T(8,128)(2,1)S(1)}, bf16[256,512]{0,1:T(8,128)(2,1)S(1)}, u32[]{:S(2)}, u32[]{:S(2)}) collective-permute-start(bf16[256,512]{0,1:T(8,128)(2,1)S(1)} %collective-permute-done.10), channel_id=1, source_target_pairs={{0,2},{2,4},{4,6},{6,8},{8,10},{10,12},{12,14},{14,16},{16,18},{18... | collective-permute-start | bytes 786440 | tf_op jit(solution)/shard_map/ppermute | solution.py:93
  166.4 0.7 copy-start.4
  167.1 10.0 %collective-permute-start.12 = (bf16[256,512]{0,1:T(8,128)(2,1)S(1)}, bf16[256,512]{0,1:T(8,128)(2,1)S(1)}, u32[]{:S(2)}, u32[]{:S(2)}) collective-permute-start(bf16[256,512]{0,1:T(8,128)(2,1)S(1)} %collective-permute-done.11), channel_id=1, source_target_pairs={{0,2},{2,4},{4,6},{6,8},{8,10},{10,12},{12,14},{14,16},{16,18},{18... | collective-permute-start | bytes 786440 | tf_op jit(solution)/shard_map/ppermute | solution.py:93
  177.1 0.7 copy-start.6
  177.8 10.1 %collective-permute-start.13 = (bf16[256,512]{0,1:T(8,128)(2,1)S(1)}, bf16[256,512]{0,1:T(8,128)(2,1)}, u32[]{:S(2)}, u32[]{:S(2)}) collective-permute-start(bf16[256,512]{0,1:T(8,128)(2,1)S(1)} %collective-permute-done.12), channel_id=1, source_target_pairs={{0,2},{2,4},{4,6},{6,8},{8,10},{10,12},{12,14},{14,16},{16,18},{18... | collective-permute-start | bytes 786440 | tf_op jit(solution)/shard_map/ppermute | solution.py:93
  187.8 47.7 %collective-permute-start.14 = (bf16[256,512]{0,1:T(8,128)(2,1)}, bf16[256,512]{0,1:T(8,128)(2,1)}, u32[]{:S(2)}, u32[]{:S(2)}) collective-permute-start(bf16[256,512]{0,1:T(8,128)(2,1)} %collective-permute-done.13), channel_id=1, source_target_pairs={{0,2},{2,4},{4,6},{6,8},{8,10},{10,12},{12,14},{14,16},{16,18},{18... | collective-permute-start | bytes 786440 | tf_op jit(solution)/shard_map/ppermute | solution.py:93
  191.1 51.9 %copy-start.5 = (bf16[256,512]{0,1:T(8,128)(2,1)S(1)}, bf16[256,512]{0,1:T(8,128)(2,1)}, u32[]{:S(2)}) copy-start(bf16[256,512]{0,1:T(8,128)(2,1)} %copy-done.4) | copy-start | bytes 786436
  191.1 51.9 %copy-start.3 = (bf16[256,512]{0,1:T(8,128)(2,1)S(1)}, bf16[256,512]{0,1:T(8,128)(2,1)}, u32[]{:S(2)}) copy-start(bf16[256,512]{0,1:T(8,128)(2,1)} %copy-done.2) | copy-start | bytes 786436
  192.4 50.5 %copy-start.7 = (bf16[256,512]{0,1:T(8,128)(2,1)S(1)}, bf16[256,512]{0,1:T(8,128)(2,1)}, u32[]{:S(2)}) copy-start(bf16[256,512]{0,1:T(8,128)(2,1)} %copy-done.6) | copy-start | bytes 786436
  242.9 2.9 copy-start.9
  270.1 31.1 %copy-start.1 = (bf16[128,2048]{1,0:T(8,128)(2,1)S(1)}, bf16[128,2048]{1,0:T(8,128)(2,1)}, u32[]{:S(2)}) copy-start(bf16[128,2048]{1,0:T(8,128)(2,1)} %param.16) | copy-start | bytes 1572868
  270.1 31.1 %copy-start.8 = (f32[2048]{0:T(1024)S(1)}, f32[2048]{0:T(1024)}, u32[]{:S(2)}) copy-start(f32[2048]{0:T(1024)} %param.23) | copy-start | bytes 24580
  270.1 32.5 %copy-start.10 = (f32[2048]{0:T(1024)S(1)}, f32[2048]{0:T(1024)}, u32[]{:S(2)}) copy-start(f32[2048]{0:T(1024)} %param.24) | copy-start | bytes 24580
  275.0 40.2 %all-gather.9.cloned.1.call-start = ((), (), s32[]{:S(2)}) async-start(), calls=%async_computation.4 | async-start | bytes 1572864 | tf_op jit(solution)/shard_map/all_gather | solution.py:128
  304.9 126.5 %all-gather.11.cloned.1.call-start = ((), (), s32[]{:S(2)}) async-start(), calls=%async_computation.5 | async-start | bytes 8912896 | tf_op jit(solution)/shard_map/all_gather | solution.py:37
  305.4 239.1 %all-gather.13.cloned.1.call-start = ((), (), s32[]{:S(2)}) async-start(), calls=%async_computation.6 | async-start | bytes 8912896 | tf_op jit(solution)/shard_map/all_gather | solution.py:38
  306.0 381.1 %all-gather.15.cloned.1.call-start = ((), (), s32[]{:S(2)}) async-start(), calls=%async_computation.7 | async-start | bytes 8912896 | tf_op jit(solution)/shard_map/all_gather | solution.py:39
  306.6 399.4 %reduce-scatter.5.cloned.1.call-start = ((), (), s32[]{:S(2)}) async-start(), calls=%async_computation.8 | async-start | bytes 1572864 | tf_op jit(solution)/shard_map/reduce_scatter | solution.py:134
  315.3 371.8 %copy-start.11 = (bf16[256,2048]{1,0:T(8,128)(2,1)S(1)}, bf16[256,2048]{1,0:T(8,128)(2,1)}, u32[]{:S(2)}) copy-start(bf16[256,2048]{1,0:T(8,128)(2,1)} %all-gather.9.cloned.1.call-done) | copy-start | bytes 3145732
  438.8 267.2 %copy-start = (bf16[128,2048]{1,0:T(8,128)(2,1)S(1)}, bf16[128,2048]{1,0:T(8,128)(2,1)}, u32[]{:S(2)}) copy-start(bf16[128,2048]{1,0:T(8,128)(2,1)} %reduce-scatter.3.cloned.1.call-done) | copy-start | bytes 1572868
Sparse Core Ops, SparseCore 0:
  22.9 97.2 all-gather.6
  275.2 24.7 reduce-scatter.2
  305.0 10.2 all-gather.8
  317.9 113.4 all-gather.10
  434.0 110.4 all-gather.12
  547.1 139.9 all-gather.14
  699.4 6.5 reduce-scatter.4
